TPU v7x, 32 devices: a whole 2x2x4 slice. The times are simulated.
32 devices in a mesh: sp: 4 (over z), fs: 4 (over y, x), tp: 2 (over core).
Axes of the slice: x: 2, y: 2, z: 4, core: 2. Of those that a mesh axis runs over, the one named last changes fastest.
Arguments:
- tokens: bfloat16 [4, 512, 2048], P('fs', ('sp', 'tp')), may hold values from -6 to 6
- input_norm_gain: float32 [2048], replicated, may hold values from 0.1 to 1.9
- pooling_input_weight: bfloat16 [2048, 1024], P('sp', 'tp'), may hold values from -0.125 to 0.125
- query_weight: bfloat16 [2048, 1024], P('sp', 'tp'), may hold values from -0.125 to 0.125
- forget_weight: bfloat16 [2048, 1024], P('sp', 'tp'), may hold values from -0.125 to 0.125
- value_weight: bfloat16 [2048, 1024], P('sp', 'tp'), may hold values from -0.125 to 0.125
- pooling_group_maps: bfloat16 [4, 256, 256], P('tp'), may hold values from -0.375 to 0.375
- pooling_scale: float32 [1024], P('tp'), may hold values from 0.1 to 1.9
- lower_bound_logits: float32 [1024], P('tp')
- decay_spike: float32 [4, 512, 8], P('fs', 'sp', 'tp'), may hold values from -0.75 to 0
- head_norm_gain: float32 [1024], P('tp'), may hold values from 0.1 to 1.9
- pooling_output_weight: bfloat16 [1024, 2048], P('tp', 'sp'), may hold values from -0.125 to 0.125
- recurrent_output_weight: bfloat16 [1024, 2048], P('tp', 'sp'), may hold values from -0.125 to 0.125
Outputs:
- mixed: bfloat16 [4, 512, 2048], P('fs', ('sp', 'tp'))
All inputs are finite; a program needn't handle non-finite values.
Results may differ from a plain program's by a relative error of at most 0.013.
Values may be sent and summed in bfloat16 or wider, within the bound.
No kernel may reach another device: no remote copies, remote signals or barrier semaphores. Data moves between devices by JAX's collectives and lax.ppermute only.
A program may use at most 64 MiB of HBM per device.

v0:
```python
import jax
import jax.numpy as jnp
from jax import lax
from jax.sharding import PartitionSpec as P

BLOCK = 64
EPSILON = 1e-06
HIGHEST = lax.Precision.HIGHEST


def shifted(value, axis, steps):
    count = lax.axis_size(axis)
    first, last = (max(0, -steps), min(count, count - steps))
    return lax.ppermute(value, axis, [(source, source + steps) for source in range(first, last)])


def entering(shard, axis, join, neutral):
    place = lax.axis_index(axis)
    gathered = jax.tree.map(
        lambda a, kind: lax.all_gather(a.astype(kind), axis), shard, (jnp.bfloat16, jnp.bfloat16)
    )
    state = jax.tree.map(lambda a, e: jnp.zeros_like(a) + jnp.asarray(e, a.dtype), shard, neutral)

    def one(step, state):
        return join(
            state,
            jax.tree.map(
                lambda a, own: lax.dynamic_index_in_dim(a, step, 0, False).astype(own.dtype),
                gathered,
                shard,
            ),
        )

    return lax.fori_loop(0, place, one, state)


def rms_scale(values, gain):
    return values * lax.rsqrt(jnp.mean(values * values, axis=-1, keepdims=True) + EPSILON) * gain


def join_state(earlier, later):
    decay_one, state_one = earlier
    decay_two, state_two = later
    return (decay_one * decay_two, decay_two[..., None] * state_one + state_two)


def body(
    tokens,
    input_norm_gain,
    pooling_input_weight,
    query_weight,
    forget_weight,
    value_weight,
    pooling_group_maps,
    pooling_scale,
    lower_bound_logits,
    decay_spike,
    head_norm_gain,
    pooling_output_weight,
    recurrent_output_weight,
):
    gathered = lax.all_gather(tokens, "tp", axis=1, tiled=True)[0]
    length_total = gathered.shape[0]
    normed = rms_scale(gathered.astype(jnp.float32), input_norm_gain).astype(jnp.bfloat16)
    pool_width = pooling_input_weight.shape[1]
    rec_width = query_weight.shape[1]
    stacked = jnp.concatenate(
        [pooling_input_weight, query_weight, forget_weight, value_weight], axis=1
    )
    out_local = jnp.concatenate([pooling_output_weight, recurrent_output_weight], axis=0)
    groups_fs = lax.axis_size("fs")
    member = lax.axis_index("fs")
    slice_width = stacked.shape[1] // groups_fs
    own_slice = lax.dynamic_slice_in_dim(stacked, member * slice_width, slice_width, 1)
    column_part = lax.all_gather(own_slice, "sp", axis=0, tiled=True)
    full_input = lax.all_gather(column_part, "fs", axis=1, tiled=True)
    projected = jnp.dot(normed, full_input, preferred_element_type=jnp.float32)
    slice_height = out_local.shape[0] // groups_fs
    own_rows = lax.dynamic_slice_in_dim(out_local, member * slice_height, slice_height, 0)
    row_part = lax.all_gather(own_rows, "sp", axis=1, tiled=True)
    out_full = lax.all_gather(row_part, "fs", axis=0, tiled=True)
    rounded = lax.optimization_barrier(projected.astype(jnp.bfloat16))
    pool_input = rounded[:, :pool_width]
    query_matrix = rounded[:, pool_width : pool_width + rec_width].astype(jnp.float32)
    forget_gate_logit = rounded[:, pool_width + rec_width : pool_width + 2 * rec_width].astype(
        jnp.float32
    )
    value_projected = rounded[:, pool_width + 2 * rec_width :].astype(jnp.float32)
    groups_local = pooling_group_maps.shape[0]
    group_size = pooling_group_maps.shape[1]
    reach_rows = 2 ** (groups_local * lax.axis_size("tp"))
    previous = shifted(pool_input[length_total - reach_rows :], "sp", 1)
    extended = jnp.concatenate([previous, pool_input], axis=0).astype(jnp.float32)
    extended = extended.reshape(reach_rows + length_total, groups_local, group_size)
    group_ids = lax.axis_index("tp") * groups_local + jnp.arange(groups_local, dtype=jnp.int32)
    windows = jnp.left_shift(jnp.int32(2), group_ids)
    window_sum = jnp.zeros((length_total, groups_local, group_size), jnp.float32)
    for offset in range(reach_rows):
        inside = (offset < windows).astype(jnp.float32)
        window_sum = (
            window_sum
            + extended[reach_rows - offset : reach_rows - offset + length_total] * inside[:, None]
        )
    position_index = lax.axis_index("sp") * length_total + jnp.arange(length_total, dtype=jnp.int32)
    counts = jnp.minimum(position_index[:, None] + 1, windows[None, :]).astype(jnp.float32)
    pool_diff = (window_sum / counts[:, :, None] - extended[reach_rows:]).astype(jnp.bfloat16)
    pool_mapped = jnp.einsum(
        "tgc,gcd->tgd", pool_diff, pooling_group_maps, preferred_element_type=jnp.float32
    )
    pool_out = (pool_mapped.reshape(length_total, pool_width) * pooling_scale).astype(jnp.bfloat16)
    local_heads = decay_spike.shape[2]
    head_width = rec_width // local_heads
    blocks = length_total // BLOCK
    block_layout = (blocks, BLOCK, local_heads, head_width)
    reader = jax.nn.silu(query_matrix).reshape(block_layout)
    key_gate_value = jax.nn.sigmoid(-lower_bound_logits) * jax.nn.sigmoid(-forget_gate_logit)
    decay_logarithm = (
        jnp.log1p(-key_gate_value).reshape(length_total, local_heads, head_width)
        + decay_spike[0][:, :, None]
    ).reshape(block_layout)
    key_rows = key_gate_value.reshape(block_layout)
    value_rows = value_projected.reshape(block_layout)
    inner_log = jnp.cumsum(decay_logarithm, axis=1)
    read_scaled = reader * jnp.exp(inner_log)
    key_scaled = key_rows * jnp.exp(-inner_log)
    causal = (jnp.arange(BLOCK)[:, None] >= jnp.arange(BLOCK)[None, :]).astype(jnp.float32)
    scores = jnp.einsum("nthd,nshd->nhts", read_scaled, key_scaled, precision=HIGHEST) * causal
    within = jnp.einsum("nhts,nshe->nthe", scores, value_rows, precision=HIGHEST)
    closing = inner_log[:, -1]
    key_tail = key_rows * jnp.exp(closing[:, None] - inner_log)
    deltas = jnp.einsum("nshd,nshe->nhde", key_tail, value_rows, precision=HIGHEST)
    block_decay = jnp.exp(closing)

    def advance(carried, input_batch):
        decay_now, delta_now = input_batch
        return (decay_now[..., None] * carried + delta_now, carried)

    initial = jnp.zeros((local_heads, head_width, head_width), jnp.float32)
    device_state, entry_states = lax.scan(advance, initial, (block_decay, deltas))
    device_decay = jnp.exp(jnp.sum(closing, axis=0))
    scanned = entering(
        (device_decay, device_state),
        "sp",
        join_state,
        (jnp.ones_like(device_decay), jnp.zeros_like(device_state)),
    )
    prior_state = scanned[1]
    before = jnp.cumsum(closing, axis=0) - closing
    start_states = entry_states + jnp.exp(before)[..., None] * prior_state[None]
    read_out = within + jnp.einsum("nthd,nhde->nthe", read_scaled, start_states, precision=HIGHEST)
    read_out = read_out.reshape(length_total, local_heads, head_width)
    recurrent_output = (
        rms_scale(read_out, 1.0).reshape(length_total, rec_width) * head_norm_gain
    ).astype(jnp.bfloat16)
    mixed_rows = jnp.concatenate([pool_out, recurrent_output], axis=1)
    summed = lax.psum_scatter(
        jnp.dot(mixed_rows, out_full, preferred_element_type=jnp.float32).astype(jnp.bfloat16),
        "tp",
        scatter_dimension=0,
        tiled=True,
    )
    return summed[None]


def solution(mesh):
    placed = (
        P("fs", ("sp", "tp"), None),
        P(),
        P("sp", "tp"),
        P("sp", "tp"),
        P("sp", "tp"),
        P("sp", "tp"),
        P("tp", None, None),
        P("tp"),
        P("tp"),
        P("fs", "sp", "tp"),
        P("tp"),
        P("tp", "sp"),
        P("tp", "sp"),
    )
    return jax.shard_map(
        body, mesh=mesh, in_specs=placed, out_specs=P("fs", ("sp", "tp"), None), check_vma=False
    )
```

profile of v0, /device:TPU:0, one launch (start us, length us, event | category | flops | bytes accessed | tf_op | source)
XLA Modules:
  0.0 247.2 jit_solution(11630460486678041191)
XLA Ops:
  6.5 0.0 copy-start
  6.5 0.0 copy-start.5
  6.5 0.0 copy-start.1
  6.5 0.0 copy-start.6
  6.5 0.0 all-gather.8.cloned.1.call-start
  6.6 0.0 copy-start.2
  6.6 2.3 fusion.8
  8.9 0.0 all-gather.8.cloned.1.call-update
  8.9 0.0 all-gather.12.cloned.1.call-start
  9.0 1.8 fusion.17
  10.8 0.0 all-gather.12.cloned.1.call-update
  10.9 0.0 all-gather.10.cloned.1.call-start
  10.9 46.6 %all-gather.8.cloned.1.call-done = bf16[2048,512]{1,0:T(8,128)(2,1)} async-done(((bf16[512,512]{1,0:T(8,128)(2,1)}), bf16[2048,512]{1,0:T(8,128)(2,1)}) %all-gather.8.cloned.1.call-update) | async-done | bytes 2097168 | tf_op jit(solution)/shard_map/all_gather | solution.py:75
  57.5 0.0 all-gather.10.cloned.1.call-update
  57.5 0.0 all-gather.14.cloned.1.call-start
  57.6 0.0 copy-done.5
  57.6 0.1 copy.116
  57.9 0.0 copy-done.1
  57.9 2.2 all_gather.25
  60.1 0.2 fusion.2
  60.3 0.1 minimum_convert_fusion
  60.3 0.0 copy-done.6
  60.3 25.6 %all-gather.12.cloned.1.call-done = bf16[256,2048]{1,0:T(8,128)(2,1)} async-done(((bf16[256,512]{1,0:T(8,128)(2,1)}), bf16[256,2048]{1,0:T(8,128)(2,1)}) %all-gather.12.cloned.1.call-update) | async-done | bytes 1048592 | tf_op jit(solution)/shard_map/all_gather | solution.py:80
  85.9 0.0 all-gather.14.cloned.1.call-update
  85.9 0.0 reduce-scatter.2.cloned.1.call-start
  86.0 88.5 %all-gather.10.cloned.1.call-done = bf16[2048,2048]{1,0:T(8,128)(2,1)} async-done(((bf16[2048,512]{1,0:T(8,128)(2,1)}), bf16[2048,2048]{1,0:T(8,128)(2,1)}) %all-gather.10.cloned.1.call-update) | async-done | bytes 8388624 | tf_op jit(solution)/shard_map/all_gather | solution.py:76
  174.5 0.0 copy-done.2
  174.5 4.7 %convolution_convert_fusion = bf16[128,2048]{1,0:T(8,128)(2,1)S(1)} fusion(bf16[2048,2048]{1,0:T(8,128)(2,1)} %all-gather.10.cloned.1.call-done, bf16[1,128,2048]{2,1,0:T(8,128)(2,1)S(1)} %all_gather.25, f32[2048]{0:T(1024)S(1)} %copy-done.2, f32[128]{0:T(128)S(1)} %add_rsqrt_fusion.1), kind=kOutput, calls=%fused_computation.5 | convolution fusion | flops 1075052544 | bytes 9445888 | tf_op jit(solution)/shard_map/dot_general | solution.py:77
  179.2 3.4 %collective-permute-start = (bf16[16,512]{1,0:T(8,128)(2,1)S(1)}, bf16[16,512]{1,0:T(8,128)(2,1)S(1)}, u32[]{:S(2)}, u32[]{:S(2)}) collective-permute-start(bf16[16,512]{1,0:T(8,128)(2,1)S(1)} %slice.154), channel_id=1, source_target_pairs={{0,8},{8,16},{16,24},{1,9},{9,17},{17,25},{2,10},{10,18},{18,26},{... | collective-permute-start | bytes 49160 | tf_op jit(solution)/shard_map/ppermute | solution.py:14
  182.6 0.2 negate_log-plus-one_fusion
  182.8 0.1 reshape.233
  182.9 0.1 reshape.232
  183.0 0.1 reshape.234
  183.2 0.2 fusion.46
  183.4 0.2 exponential_multiply_fusion
  183.6 0.6 fusion.41
  184.2 0.5 while.26
  184.3 0.2 bitcast_add_fusion.2
  184.5 0.2 bitcast_add_fusion.2
  184.8 9.1 %all-gather.2 = bf16[4,4,128]{2,1,0:T(4,128)(2,1)S(1)} all-gather(bf16[1,4,128]{2,1,0:T(4,128)(2,1)S(1)} %fusion.57), channel_id=2, replica_groups=mesh['sp'=4,'fs'=4,'tp'=2] {'sp'}, dimensions={0}, use_global_device_ids=true | all-gather | bytes 5120 | tf_op jit(solution)/shard_map/all_gather | solution.py:20
  193.8 14.9 %all-gather.1 = bf16[16,128,128]{2,1,0:T(8,128)(2,1)S(1)} all-gather(bf16[4,128,128]{2,1,0:T(8,128)(2,1)S(1)} %convert_element_type.223), channel_id=3, replica_groups=mesh['sp'=4,'fs'=4,'tp'=2] {'sp'}, dimensions={0}, use_global_device_ids=true | all-gather | bytes 655360 | tf_op jit(solution)/shard_map/all_gather | solution.py:20
  208.7 0.0 copy-start.3
  208.7 0.5 convolution_multiply_fusion
  209.3 0.3 fusion.54
  209.6 0.8 multiply_reduce_fusion
  210.4 0.3 copy.117
  210.7 0.3 reshape.244
  211.0 0.1 rsqrt.21
  211.1 0.0 copy-done.3
  211.1 0.1 fusion.39
  211.2 0.0 collective-permute-done
  211.3 0.5 fusion.61
  211.8 0.0 copy-start.4
  211.8 0.0 copy-done
  211.8 0.5 convolution_bitcast_fusion
  212.3 0.1 copy.105
  212.4 0.0 copy-done.4
  212.4 0.1 fusion.40
  212.6 16.2 %all-gather.14.cloned.1.call-done = bf16[1024,2048]{1,0:T(8,128)(2,1)} async-done(((bf16[256,2048]{1,0:T(8,128)(2,1)}), bf16[1024,2048]{1,0:T(8,128)(2,1)}) %all-gather.14.cloned.1.call-update) | async-done | bytes 4194320 | tf_op jit(solution)/shard_map/all_gather | solution.py:81
  228.8 3.7 %convolution_convert_fusion.1 = bf16[128,2048]{1,0:T(8,128)(2,1)} fusion(bf16[1024,2048]{1,0:T(8,128)(2,1)} %all-gather.14.cloned.1.call-done, bf16[128,512]{0,1:T(8,128)(2,1)S(1)} %fusion.39, bf16[128,512]{0,1:T(8,128)(2,1)S(1)} %fusion.40), kind=kOutput, calls=%fused_computation.6 | convolution fusion | flops 537657344 | bytes 4980736 | tf_op jit(solution)/shard_map/dot_general | solution.py:157
  232.5 0.0 reduce-scatter.2.cloned.1.call-update
  232.5 8.1 %reduce-scatter.2.cloned.1.call-done = bf16[64,2048]{1,0:T(8,128)(2,1)} async-done(((bf16[128,2048]{1,0:T(8,128)(2,1)}), bf16[64,2048]{1,0:T(8,128)(2,1)}) %reduce-scatter.2.cloned.1.call-update) | async-done | bytes 262160 | tf_op jit(solution)/shard_map/reduce_scatter | solution.py:156
  (32 shorter events, 0.3 us)
Async XLA Ops:
  6.5 205.2 %copy-start = (bf16[2,256,256]{2,1,0:T(8,128)(2,1)S(1)}, bf16[2,256,256]{2,1,0:T(8,128)(2,1)}, u32[]{:S(2)}) copy-start(bf16[2,256,256]{2,1,0:T(8,128)(2,1)} %param.23) | copy-start | bytes 786436
  6.5 51.1 %copy-start.5 = (f32[1,128,4]{1,2,0:T(4,128)S(1)}, f32[1,128,4]{1,2,0:T(4,128)}, u32[]{:S(2)}) copy-start(f32[1,128,4]{1,2,0:T(4,128)} %param.26) | copy-start | bytes 6148
  6.5 51.3 %copy-start.1 = (bf16[1,64,2048]{2,1,0:T(8,128)(2,1)S(1)}, bf16[1,64,2048]{2,1,0:T(8,128)(2,1)}, u32[]{:S(2)}) copy-start(bf16[1,64,2048]{2,1,0:T(8,128)(2,1)} %param.17) | copy-start | bytes 786436
  6.5 53.8 %copy-start.6 = (f32[512]{0:T(512)S(1)}, f32[512]{0:T(512)}, u32[]{:S(2)}) copy-start(f32[512]{0:T(512)} %param.25) | copy-start | bytes 6148
  6.5 51.0 %all-gather.8.cloned.1.call-start = ((), (), s32[]{:S(2)}) async-start(), calls=%async_computation.1 | async-start | bytes 2621440 | tf_op jit(solution)/shard_map/all_gather | solution.py:75
  6.6 167.9 %copy-start.2 = (f32[2048]{0:T(1024)S(1)}, f32[2048]{0:T(1024)}, u32[]{:S(2)}) copy-start(f32[2048]{0:T(1024)} %param.18) | copy-start | bytes 24580
  8.9 77.0 %all-gather.12.cloned.1.call-start = ((), (), s32[]{:S(2)}) async-start(), calls=%async_computation.3 | async-start | bytes 1310720 | tf_op jit(solution)/shard_map/all_gather | solution.py:80
  10.9 163.6 %all-gather.10.cloned.1.call-start = ((), (), s32[]{:S(2)}) async-start(), calls=%async_computation.2 | async-start | bytes 10485760 | tf_op jit(solution)/shard_map/all_gather | solution.py:76
  57.5 171.3 %all-gather.14.cloned.1.call-start = ((), (), s32[]{:S(2)}) async-start(), calls=%async_computation.4 | async-start | bytes 5242880 | tf_op jit(solution)/shard_map/all_gather | solution.py:81
  85.9 154.7 %reduce-scatter.2.cloned.1.call-start = ((), (), s32[]{:S(2)}) async-start(), calls=%async_computation.5 | async-start | bytes 786432 | tf_op jit(solution)/shard_map/reduce_scatter | solution.py:156
  179.2 32.0 %collective-permute-start = (bf16[16,512]{1,0:T(8,128)(2,1)S(1)}, bf16[16,512]{1,0:T(8,128)(2,1)S(1)}, u32[]{:S(2)}, u32[]{:S(2)}) collective-permute-start(bf16[16,512]{1,0:T(8,128)(2,1)S(1)} %slice.154), channel_id=1, source_target_pairs={{0,8},{8,16},{16,24},{1,9},{9,17},{17,25},{2,10},{10,18},{18,26},{... | collective-permute-start | bytes 49160 | tf_op jit(solution)/shard_map/ppermute | solution.py:14
  208.7 2.4 copy-start.3
  211.8 0.7 copy-start.4
Sparse Core Ops, SparseCore 0:
  9.1 48.4 all-gather.7
  59.1 26.7 all-gather.11
  87.7 86.7 all-gather.9
  176.2 52.5 all-gather.13
  232.7 7.9 reduce-scatter.1
where the time goes:
time: 247 us
  waiting for transfers between devices  185 us (75%)
  blocking collectives  26.1 us (11%)
  between operations  13.5 us (5%)
  matrix products  11.1 us (4%)
  other arithmetic  5.86 us (2%)
  starting transfers between devices  3.58 us (1%)
    all_gather x1, waiting for transfers between devices, body(): full_input = lax.all_gather(column_part, 'fs', axis=1, tiled=True)  88.5 us
    all_gather x1, waiting for transfers between devices, body(): column_part = lax.all_gather(own_slice, 'sp', axis=0, tiled=True)  46.6 us
    all_gather x1, waiting for transfers between devices, body(): row_part = lax.all_gather(own_rows, 'sp', axis=1, tiled=True)  25.6 us
    all_gather x2, blocking collectives, entering(): lax.all_gather(a.astype(kind), axis)  23.9 us
    all_gather x1, waiting for transfers between devices, body(): out_full = lax.all_gather(row_part, 'fs', axis=0, tiled=True)  16.2 us
    reduce_scatter x1, waiting for transfers between devices, body(): lax.psum_scatter(jnp.dot(mixed_rows, out_full, preferred_element_type=jnp...  8.08 us
  transfers between devices with their start and end apart: 6, of which 5 were waited for; matrix products, arithmetic and copies ran while one was open for 5% of the time, Pallas kernels for 0%

commit v1 on v0

--- a/solution.py
+++ b/solution.py
@@ -72,7 +72,12 @@
     member = lax.axis_index("fs")
     slice_width = stacked.shape[1] // groups_fs
     own_slice = lax.dynamic_slice_in_dim(stacked, member * slice_width, slice_width, 1)
-    column_part = lax.all_gather(own_slice, "sp", axis=0, tiled=True)
+    ring = [own_slice]
+    for hop in range(3):
+        ring.append(lax.ppermute(ring[-1], "sp", [(dev, (dev + 1) % 4) for dev in range(4)]))
+    column_part = jnp.roll(
+        jnp.concatenate(ring[::-1], axis=0), (lax.axis_index("sp") + 1) * ring[0].shape[0], axis=0
+    )
     full_input = lax.all_gather(column_part, "fs", axis=1, tiled=True)
     projected = jnp.dot(normed, full_input, preferred_element_type=jnp.float32)
     slice_height = out_local.shape[0] // groups_fs

time: 247 us -> 233 us (0.943)
  waiting for transfers between devices: 185 us -> 166 us
  starting transfers between devices: 3.58 us -> 6.62 us
    all_gather x1 -> x0, waiting for transfers between devices: 46.6 us -> none  [body(): column_part = lax.all_gather(own_slice, 'sp', axis=0, tiled=True)]
    ppermute x0 -> x3, waiting for transfers between devices: none -> 41 us  [body(): lax.ppermute(ring[-1], 'sp', [(dev, (dev + 1) % 4) for dev in range(4)])]
    all_gather x1, waiting for transfers between devices: 25.6 us -> 12.4 us  [body(): row_part = lax.all_gather(own_rows, 'sp', axis=1, tiled=True)]
    ppermute x0 -> x3, starting transfers between devices: none -> 3.11 us  [body(): lax.ppermute(ring[-1], 'sp', [(dev, (dev + 1) % 4) for dev in range(4)])]
  transfers between devices with their start and end apart: 6 -> 8, of which waited for: 5 -> 7; matrix products, arithmetic and copies ran while one was open for 5% -> 6% of each run, Pallas kernels for 0% -> 0%
where the time goes in v1:
time: 233 us
  waiting for transfers between devices  166 us (71%)
  blocking collectives  26.1 us (11%)
  between operations  13.6 us (6%)
  matrix products  11.1 us (5%)
  starting transfers between devices  6.62 us (3%)
  other arithmetic  5.02 us (2%)
  local copies, waits for them, and re-layouts  3.58 us (2%)
    all_gather x1, waiting for transfers between devices, body(): full_input = lax.all_gather(column_part, 'fs', axis=1, tiled=True)  88.5 us
    ppermute x3, waiting for transfers between devices, body(): lax.ppermute(ring[-1], 'sp', [(dev, (dev + 1) % 4) for dev in range(4)])  41 us
    all_gather x2, blocking collectives, entering(): lax.all_gather(a.astype(kind), axis)  23.9 us
    all_gather x1, waiting for transfers between devices, body(): out_full = lax.all_gather(row_part, 'fs', axis=0, tiled=True)  16.4 us
    all_gather x1, waiting for transfers between devices, body(): row_part = lax.all_gather(own_rows, 'sp', axis=1, tiled=True)  12.4 us
    reduce_scatter x1, waiting for transfers between devices, body(): lax.psum_scatter(jnp.dot(mixed_rows, out_full, preferred_element_type=jnp...  8.08 us
    dot_general x1, matrix products, body(): projected = jnp.dot(normed, full_input, preferred_element_type=jnp.float32)  4.69 us
  transfers between devices with their start and end apart: 8, of which 7 were waited for; matrix products, arithmetic and copies ran while one was open for 6% of the time, Pallas kernels for 0%

profile of v1, /device:TPU:0, one launch (start us, length us, event | category | flops | bytes accessed | tf_op | source)
XLA Modules:
  0.0 232.6 jit_solution(1903592280309313660)
XLA Ops:
  6.5 0.0 copy-start
  6.5 0.0 all-gather.9.cloned.1.call-start
  6.5 1.5 fusion.8
  8.0 3.1 %collective-permute-start = (bf16[512,512]{1,0:T(8,128)(2,1)S(1)}, bf16[512,512]{1,0:T(8,128)(2,1)S(1)}, u32[]{:S(2)}, u32[]{:S(2)}) collective-permute-start(bf16[512,512]{1,0:T(8,128)(2,1)S(1)} %fusion.8), channel_id=1, source_target_pairs={{0,8},{8,16},{16,24},{24,0},{1,9},{9,17},{17,25},{25,1},{2,10},{10... | collective-permute-start | bytes 1572872 | tf_op jit(solution)/shard_map/ppermute | solution.py:77
  11.1 13.9 %collective-permute-done = bf16[512,512]{1,0:T(8,128)(2,1)S(1)} collective-permute-done((bf16[512,512]{1,0:T(8,128)(2,1)S(1)}, bf16[512,512]{1,0:T(8,128)(2,1)S(1)}, u32[]{:S(2)}, u32[]{:S(2)}) %collective-permute-start) | collective-permute-done | bytes 524320 | tf_op jit(solution)/shard_map/ppermute | solution.py:77
  25.1 0.0 collective-permute-start.1
  25.1 14.9 %collective-permute-done.1 = bf16[512,512]{1,0:T(8,128)(2,1)S(1)} collective-permute-done((bf16[512,512]{1,0:T(8,128)(2,1)S(1)}, bf16[512,512]{1,0:T(8,128)(2,1)S(1)}, u32[]{:S(2)}, u32[]{:S(2)}) %collective-permute-start.1) | collective-permute-done | bytes 524320 | tf_op jit(solution)/shard_map/ppermute | solution.py:77
  40.0 0.0 collective-permute-start.2
  40.0 1.8 fusion.17
  41.8 0.0 all-gather.9.cloned.1.call-update
  41.8 0.0 all-gather.7.cloned.1.call-start
  41.9 12.2 %collective-permute-done.2 = bf16[512,512]{1,0:T(8,128)(2,1)S(1)} collective-permute-done((bf16[512,512]{1,0:T(8,128)(2,1)S(1)}, bf16[512,512]{1,0:T(8,128)(2,1)S(1)}, u32[]{:S(2)}, u32[]{:S(2)}) %collective-permute-start.2) | collective-permute-done | bytes 524320 | tf_op jit(solution)/shard_map/ppermute | solution.py:77
  54.3 0.0 copy-start.5
  54.3 0.0 copy-start.1
  54.4 0.0 copy-start.6
  54.4 0.0 copy-start.2
  54.5 1.5 constant_dynamic-slice_fusion
  55.9 0.0 all-gather.7.cloned.1.call-update
  56.0 0.0 all-gather.11.cloned.1.call-start
  56.0 0.0 copy-done.5
  56.0 0.1 copy.116
  56.3 0.0 copy-done.1
  56.3 2.2 all_gather.22
  58.5 0.2 fusion.2
  58.7 0.1 minimum_convert_fusion
  58.8 0.0 copy-done.6
  58.8 12.4 %all-gather.9.cloned.1.call-done = bf16[256,2048]{1,0:T(8,128)(2,1)} async-done(((bf16[256,512]{1,0:T(8,128)(2,1)}), bf16[256,2048]{1,0:T(8,128)(2,1)}) %all-gather.9.cloned.1.call-update) | async-done | bytes 1048592 | tf_op jit(solution)/shard_map/all_gather | solution.py:85
  71.2 0.0 all-gather.11.cloned.1.call-update
  71.2 0.0 reduce-scatter.2.cloned.1.call-start
  71.3 88.5 %all-gather.7.cloned.1.call-done = bf16[2048,2048]{1,0:T(8,128)(2,1)} async-done(((bf16[2048,512]{1,0:T(8,128)(2,1)}), bf16[2048,2048]{1,0:T(8,128)(2,1)}) %all-gather.7.cloned.1.call-update) | async-done | bytes 8388624 | tf_op jit(solution)/shard_map/all_gather | solution.py:81
  159.8 4.7 %convolution_convert_fusion = bf16[128,2048]{1,0:T(8,128)(2,1)S(1)} fusion(bf16[2048,2048]{1,0:T(8,128)(2,1)} %all-gather.7.cloned.1.call-done, bf16[1,128,2048]{2,1,0:T(8,128)(2,1)S(1)} %all_gather.22, f32[2048]{0:T(1024)S(1)} %copy-done.2, f32[128]{0:T(128)S(1)} %add_rsqrt_fusion.1), kind=kOutput, calls=%fused_computation.5 | convolution fusion | flops 1075052544 | bytes 9445888 | tf_op jit(solution)/shard_map/dot_general | solution.py:82
  164.5 3.4 %collective-permute-start.3 = (bf16[16,512]{1,0:T(8,128)(2,1)S(1)}, bf16[16,512]{1,0:T(8,128)(2,1)S(1)}, u32[]{:S(2)}, u32[]{:S(2)}) collective-permute-start(bf16[16,512]{1,0:T(8,128)(2,1)S(1)} %slice.154), channel_id=1, source_target_pairs={{0,8},{8,16},{16,24},{1,9},{9,17},{17,25},{2,10},{10,18},{18,26},{... | collective-permute-start | bytes 49160 | tf_op jit(solution)/shard_map/ppermute | solution.py:14
  167.9 0.2 negate_log-plus-one_fusion
  168.1 0.1 reshape.233
  168.2 0.1 reshape.232
  168.3 0.1 reshape.234
  168.5 0.2 fusion.46
  168.7 0.2 exponential_multiply_fusion
  168.9 0.6 fusion.41
  169.5 0.5 while.26
  169.6 0.2 bitcast_add_fusion.2
  169.8 0.2 bitcast_add_fusion.2
  170.1 9.1 %all-gather.2 = bf16[4,4,128]{2,1,0:T(4,128)(2,1)S(1)} all-gather(bf16[1,4,128]{2,1,0:T(4,128)(2,1)S(1)} %fusion.57), channel_id=2, replica_groups=mesh['sp'=4,'fs'=4,'tp'=2] {'sp'}, dimensions={0}, use_global_device_ids=true | all-gather | bytes 5120 | tf_op jit(solution)/shard_map/all_gather | solution.py:20
  179.1 14.9 %all-gather.1 = bf16[16,128,128]{2,1,0:T(8,128)(2,1)S(1)} all-gather(bf16[4,128,128]{2,1,0:T(8,128)(2,1)S(1)} %convert_element_type.223), channel_id=3, replica_groups=mesh['sp'=4,'fs'=4,'tp'=2] {'sp'}, dimensions={0}, use_global_device_ids=true | all-gather | bytes 655360 | tf_op jit(solution)/shard_map/all_gather | solution.py:20
  194.0 0.0 copy-start.3
  194.0 0.5 convolution_multiply_fusion
  194.6 0.3 fusion.54
  194.9 0.8 multiply_reduce_fusion
  195.7 0.3 copy.117
  196.0 0.3 reshape.244
  196.3 0.1 rsqrt.21
  196.4 0.1 fusion.39
  196.5 0.0 collective-permute-done.3
  196.5 0.5 fusion.61
  197.0 0.0 copy-start.4
  197.1 0.0 copy-done
  197.1 0.5 convolution_bitcast_fusion
  197.6 0.1 copy.105
  197.7 0.0 copy-done.4
  197.7 0.1 fusion.40
  197.9 16.4 %all-gather.11.cloned.1.call-done = bf16[1024,2048]{1,0:T(8,128)(2,1)} async-done(((bf16[256,2048]{1,0:T(8,128)(2,1)}), bf16[1024,2048]{1,0:T(8,128)(2,1)}) %all-gather.11.cloned.1.call-update) | async-done | bytes 4194320 | tf_op jit(solution)/shard_map/all_gather | solution.py:86
  214.2 3.7 %convolution_convert_fusion.1 = bf16[128,2048]{1,0:T(8,128)(2,1)} fusion(bf16[1024,2048]{1,0:T(8,128)(2,1)} %all-gather.11.cloned.1.call-done, bf16[128,512]{0,1:T(8,128)(2,1)S(1)} %fusion.39, bf16[128,512]{0,1:T(8,128)(2,1)S(1)} %fusion.40), kind=kOutput, calls=%fused_computation.6 | convolution fusion | flops 537657344 | bytes 4980736 | tf_op jit(solution)/shard_map/dot_general | solution.py:162
  218.0 0.0 reduce-scatter.2.cloned.1.call-update
  218.0 8.1 %reduce-scatter.2.cloned.1.call-done = bf16[64,2048]{1,0:T(8,128)(2,1)} async-done(((bf16[128,2048]{1,0:T(8,128)(2,1)}), bf16[64,2048]{1,0:T(8,128)(2,1)}) %reduce-scatter.2.cloned.1.call-update) | async-done | bytes 262160 | tf_op jit(solution)/shard_map/reduce_scatter | solution.py:161
  (42 shorter events, 0.6 us)
Async XLA Ops:
  6.5 190.5 %copy-start = (bf16[2,256,256]{2,1,0:T(8,128)(2,1)S(1)}, bf16[2,256,256]{2,1,0:T(8,128)(2,1)}, u32[]{:S(2)}) copy-start(bf16[2,256,256]{2,1,0:T(8,128)(2,1)} %param.23) | copy-start | bytes 786436
  6.5 64.7 %all-gather.9.cloned.1.call-start = ((), (), s32[]{:S(2)}) async-start(), calls=%async_computation.2 | async-start | bytes 1310720 | tf_op jit(solution)/shard_map/all_gather | solution.py:85
  8.0 17.1 %collective-permute-start = (bf16[512,512]{1,0:T(8,128)(2,1)S(1)}, bf16[512,512]{1,0:T(8,128)(2,1)S(1)}, u32[]{:S(2)}, u32[]{:S(2)}) collective-permute-start(bf16[512,512]{1,0:T(8,128)(2,1)S(1)} %fusion.8), channel_id=1, source_target_pairs={{0,8},{8,16},{16,24},{24,0},{1,9},{9,17},{17,25},{25,1},{2,10},{10... | collective-permute-start | bytes 1572872 | tf_op jit(solution)/shard_map/ppermute | solution.py:77
  25.1 14.9 %collective-permute-start.1 = (bf16[512,512]{1,0:T(8,128)(2,1)S(1)}, bf16[512,512]{1,0:T(8,128)(2,1)S(1)}, u32[]{:S(2)}, u32[]{:S(2)}) collective-permute-start(bf16[512,512]{1,0:T(8,128)(2,1)S(1)} %collective-permute-done), channel_id=1, source_target_pairs={{0,8},{8,16},{16,24},{24,0},{1,9},{9,17},{17,25},{25,1},{2,10},{10... | collective-permute-start | bytes 1572872 | tf_op jit(solution)/shard_map/ppermute | solution.py:77
  40.0 14.1 %collective-permute-start.2 = (bf16[512,512]{1,0:T(8,128)(2,1)S(1)}, bf16[512,512]{1,0:T(8,128)(2,1)S(1)}, u32[]{:S(2)}, u32[]{:S(2)}) collective-permute-start(bf16[512,512]{1,0:T(8,128)(2,1)S(1)} %collective-permute-done.1), channel_id=1, source_target_pairs={{0,8},{8,16},{16,24},{24,0},{1,9},{9,17},{17,25},{25,1},{2,10},{10... | collective-permute-start | bytes 1572872 | tf_op jit(solution)/shard_map/ppermute | solution.py:77
  41.8 118.0 %all-gather.7.cloned.1.call-start = ((), (), s32[]{:S(2)}) async-start(), calls=%async_computation.1 | async-start | bytes 10485760 | tf_op jit(solution)/shard_map/all_gather | solution.py:81
  54.3 1.7 copy-start.5
  54.3 2.0 copy-start.1
  54.4 4.4 %copy-start.6 = (f32[512]{0:T(512)S(1)}, f32[512]{0:T(512)}, u32[]{:S(2)}) copy-start(f32[512]{0:T(512)} %param.25) | copy-start | bytes 6148
  54.4 105.3 %copy-start.2 = (f32[2048]{0:T(1024)S(1)}, f32[2048]{0:T(1024)}, u32[]{:S(2)}) copy-start(f32[2048]{0:T(1024)} %param.18) | copy-start | bytes 24580
  56.0 158.3 %all-gather.11.cloned.1.call-start = ((), (), s32[]{:S(2)}) async-start(), calls=%async_computation.3 | async-start | bytes 5242880 | tf_op jit(solution)/shard_map/all_gather | solution.py:86
  71.2 154.9 %reduce-scatter.2.cloned.1.call-start = ((), (), s32[]{:S(2)}) async-start(), calls=%async_computation.4 | async-start | bytes 786432 | tf_op jit(solution)/shard_map/reduce_scatter | solution.py:161
  164.5 32.0 %collective-permute-start.3 = (bf16[16,512]{1,0:T(8,128)(2,1)S(1)}, bf16[16,512]{1,0:T(8,128)(2,1)S(1)}, u32[]{:S(2)}, u32[]{:S(2)}) collective-permute-start(bf16[16,512]{1,0:T(8,128)(2,1)S(1)} %slice.154), channel_id=1, source_target_pairs={{0,8},{8,16},{16,24},{1,9},{9,17},{17,25},{2,10},{10,18},{18,26},{... | collective-permute-start | bytes 49160 | tf_op jit(solution)/shard_map/ppermute | solution.py:14
  194.0 2.3 %copy-start.3 = (f32[512]{0:T(512)S(1)}, f32[512]{0:T(512)}, u32[]{:S(2)}) copy-start(f32[512]{0:T(512)} %param.27) | copy-start | bytes 6148
  197.0 0.7 copy-start.4
Sparse Core Ops, SparseCore 0:
  41.9 29.2 all-gather.8
  73.0 86.7 all-gather.6
  161.6 52.5 all-gather.10
  218.1 7.9 reduce-scatter.1
